TPU v7x, 128 devices: a whole 4x4x4 slice. The times are simulated.
128 devices in a mesh: pp: 4 (over x), fs: 4 (over y), tp: 8 (over z, core).
Axes of the slice: x: 4, y: 4, z: 4, core: 2. Of those that a mesh axis runs over, the one named last changes fastest.
Arguments:
- micro_in: bfloat16 [2, 96, 1024], P(None, 'pp', ('tp', 'fs')), may hold values from -6 to 6
- norm_gain: float32 [4, 1024], P('pp'), may hold values from 0.5 to 1.5
- proj_gate: bfloat16 [4, 1024, 8, 4, 64], P('pp', None, 'tp', 'fs'), may hold values from -0.1875 to 0.1875
- proj_value: bfloat16 [4, 1024, 8, 4, 64], P('pp', None, 'tp', 'fs'), may hold values from -0.1875 to 0.1875
- proj_write: bfloat16 [4, 1024, 8, 128], P('pp', None, 'tp'), may hold values from -0.1875 to 0.1875
- proj_read: bfloat16 [4, 1024, 8, 128], P('pp', None, 'tp'), may hold values from -0.1875 to 0.1875
- proj_step: bfloat16 [4, 1024, 2, 8, 4], P('pp', None, None, 'tp', 'fs'), may hold values from -0.1875 to 0.1875
- step_bias: float32 [4, 2, 8, 4], P('pp', None, 'tp', 'fs'), may hold values from -4.6 to -2.3
- decay_log: float32 [4, 2, 8, 4], P('pp', None, 'tp', 'fs'), may hold values from 0 to 2.77
- skip_gain: float32 [4, 8, 4], P('pp', 'tp', 'fs'), may hold values from 0.5 to 1.5
- conv_value: float32 [4, 5, 8, 4, 64], P('pp', None, 'tp', 'fs'), may hold values from -2.5 to 2.5
- conv_write: float32 [4, 5, 8, 128], P('pp', None, 'tp'), may hold values from -2.5 to 2.5
- conv_read: float32 [4, 5, 8, 128], P('pp', None, 'tp'), may hold values from -2.5 to 2.5
- proj_out: bfloat16 [4, 8, 4, 64, 1024], P('pp', 'tp', 'fs'), may hold values from -0.125 to 0.125
Outputs:
- mixed_out: bfloat16 [2, 96, 1024], P(None, 'pp', ('tp', 'fs'))
All inputs are finite; a program needn't handle non-finite values.
Results may differ from a plain program's by a relative error of at most 0.025.
Values may be sent and summed in bfloat16 or wider, within the bound.
No kernel may reach another device: no remote copies, remote signals or barrier semaphores. Data moves between devices by JAX's collectives and lax.ppermute only.
A program may use at most 64 MiB of HBM per device.

v0:
```python
import jax
import jax.numpy as jnp
from jax import lax
from jax.sharding import Mesh
from jax.sharding import PartitionSpec as P

TP_FS = ("tp_0", "tp_1", "fs")
TP = ("tp_0", "tp_1")
epsilon = 1e-06


def sum_in_order(parts, axes, order):
    lengths = [lax.axis_size(a) for a in axes]
    parts = parts.reshape(*lengths, *parts.shape[1:])
    parts = parts.transpose(*order, *range(len(axes), parts.ndim))
    parts = parts.reshape(-1, *parts.shape[len(axes) :])
    for k in order:
        parts = lax.psum_scatter(parts, axes[k], scatter_dimension=0, tiled=True)
    return parts[0]


def cut_along(shard, dim, peers):
    lengths = shard.shape
    parts = shard.reshape(*lengths[:dim], peers, lengths[dim] // peers, *lengths[dim + 1 :])
    return jnp.moveaxis(parts, dim, 0)


def sum_by_axis(shard, axes, order, dim):
    peers = lax.axis_size(axes)
    return sum_in_order(cut_along(shard, dim, peers), axes, order)


def own_rows_2(term, span, axes, order):
    running = term(jnp.int32(0), span * lax.axis_size(axes)).astype(jnp.bfloat16)
    return sum_by_axis(running, axes, order, 0).astype(jnp.float32)


def passed_along(shard, axis, by):
    peers = lax.axis_size(axis)
    pairs = [(i, i + by) for i in range(peers) if 0 <= i + by < peers]
    return lax.ppermute(shard, axis, pairs)


def from_root(shard, axis, root):
    return lax.dynamic_index_in_dim(lax.all_gather(shard, axis), root, 0, keepdims=False)


def total_of_pieces(shard, axis):
    return lax.all_gather(shard, axis).sum(0)


def centred_conv(signal, conv_taps):
    span_width = conv_taps.shape[0]
    half_width = span_width // 2
    length = signal.shape[0]
    padded = jnp.pad(signal, ((half_width, half_width), (0, 0)))
    running = jnp.zeros_like(signal)
    for offset in range(span_width):
        running = running + padded[offset : offset + length] * conv_taps[offset]
    return running


def duality_mix(
    gate_flat,
    value_flat,
    write_flat,
    read_flat,
    step_raw,
    step_bias,
    decay_log,
    skip_gain,
    conv_value,
    conv_write,
    conv_read,
):
    groups, per_group = skip_gain.shape
    length = gate_flat.shape[0]
    head_size = value_flat.shape[1] // (groups * per_group)
    state_size = write_flat.shape[1] // groups
    taps_count = conv_value.shape[0]
    value_act = jax.nn.silu(
        centred_conv(value_flat.astype(jnp.float32), conv_value.reshape(taps_count, -1))
    ).astype(jnp.bfloat16)
    write_act = jax.nn.silu(
        centred_conv(write_flat.astype(jnp.float32), conv_write.reshape(taps_count, -1))
    ).astype(jnp.bfloat16)
    read_act = jax.nn.silu(
        centred_conv(read_flat.astype(jnp.float32), conv_read.reshape(taps_count, -1))
    ).astype(jnp.bfloat16)
    step_size = jax.nn.softplus(step_raw.reshape(length, 2, groups, per_group) + step_bias[None])
    log_decay = step_size * (-jnp.exp(decay_log))[None]
    fwd_cum = jnp.cumsum(log_decay[:, 0], axis=0)
    bwd_cum = jnp.flip(jnp.cumsum(jnp.flip(log_decay[:, 1], 0), axis=0), 0)
    positions = jnp.arange(length)
    lower_mask = (positions[:, None] >= positions[None, :])[:, :, None, None]
    upper_mask = (positions[:, None] <= positions[None, :])[:, :, None, None]
    fwd_weight = (
        jnp.exp(jnp.where(lower_mask, fwd_cum[:, None] - fwd_cum[None, :], -jnp.inf))
        * step_size[None, :, 0]
    )
    bwd_weight = (
        jnp.exp(jnp.where(upper_mask, bwd_cum[:, None] - bwd_cum[None, :], -jnp.inf))
        * step_size[None, :, 1]
    )
    scores = jnp.einsum(
        "tgn,sgn->tsg",
        read_act.reshape(length, groups, state_size),
        write_act.reshape(length, groups, state_size),
        preferred_element_type=jnp.float32,
    )
    combined = scores[:, :, :, None] * (fwd_weight + bwd_weight)
    value_heads = value_act.reshape(length, groups, per_group, head_size).astype(jnp.float32)
    mixed_heads = jnp.einsum(
        "tsgh,sghp->tghp", combined, value_heads, precision=lax.Precision.HIGHEST
    )
    mixed_heads = mixed_heads + skip_gain[None, :, :, None] * value_heads
    return (mixed_heads.reshape(length, -1) * jax.nn.silu(gate_flat.astype(jnp.float32))).astype(
        jnp.bfloat16
    )


def per_device(
    micro_in,
    norm_gain,
    proj_gate,
    proj_value,
    proj_write,
    proj_read,
    proj_step,
    step_bias,
    decay_log,
    skip_gain,
    conv_value,
    conv_write,
    conv_read,
    proj_out,
):
    section_count = lax.axis_size("pp")
    section_idx = lax.axis_index("pp")
    width_model = norm_gain.shape[1]
    fed_blocks = lax.all_gather(micro_in, "pp", axis=1, tiled=True)
    micro_count = fed_blocks.shape[0]
    length = fed_blocks.shape[1]
    fed_columns = jnp.swapaxes(fed_blocks, 1, 2)
    gain_vec = norm_gain[0].astype(jnp.float32)
    cut_gate = proj_gate.shape[2] * proj_gate.shape[3] * proj_gate.shape[4]
    cut_write = proj_write.shape[2] * proj_write.shape[3]
    weight_all = jnp.concatenate(
        [
            proj_gate[0].reshape(width_model, -1),
            proj_value[0].reshape(width_model, -1),
            proj_write[0].reshape(width_model, -1),
            proj_read[0].reshape(width_model, -1),
            proj_step[0].reshape(width_model, -1),
        ],
        axis=1,
    )
    out_weights = proj_out[0].reshape(-1, width_model)
    own_rows = width_model // lax.axis_size(TP_FS)

    def project(column_block):
        gathered = lax.all_gather(column_block, TP_FS, axis=0, tiled=True)
        as_float = gathered.astype(jnp.float32)
        scale_rms = lax.rsqrt(jnp.mean(as_float * as_float, axis=0) + epsilon)
        normed = (as_float * scale_rms[None, :] * gain_vec[:, None]).astype(jnp.bfloat16)
        return lax.dot_general(
            normed, weight_all, (((0,), (0,)), ((), ())), preferred_element_type=jnp.float32
        )

    def term_maker(token_rows):

        def term_rows(offset, span_count):
            weight_cols = lax.dynamic_slice_in_dim(out_weights, offset, span_count, 1)
            return lax.dot_general(
                weight_cols,
                token_rows,
                (((0,), (1,)), ((), ())),
                preferred_element_type=jnp.float32,
            )

        return term_rows

    def mix_block(column_block):
        projected = project(column_block)
        gate_flat = projected[:, :cut_gate].astype(jnp.bfloat16)
        value_flat = projected[:, cut_gate : 2 * cut_gate].astype(jnp.bfloat16)
        write_flat = projected[:, 2 * cut_gate : 2 * cut_gate + cut_write].astype(jnp.bfloat16)
        read_flat = projected[:, 2 * cut_gate + cut_write : 2 * cut_gate + 2 * cut_write].astype(
            jnp.bfloat16
        )
        step_raw = projected[:, 2 * cut_gate + 2 * cut_write :]
        gated_out = duality_mix(
            gate_flat,
            value_flat,
            write_flat,
            read_flat,
            step_raw,
            step_bias[0],
            decay_log[0],
            skip_gain[0],
            conv_value[0],
            conv_write[0],
            conv_read[0],
        )
        summed = own_rows_2(term_maker(gated_out), own_rows, TP_FS, (1, 0, 2))
        branch = lax.optimization_barrier(summed.astype(jnp.bfloat16))
        return (column_block.astype(jnp.float32) + 0.5 * branch.astype(jnp.float32)).astype(
            jnp.bfloat16
        )

    total_steps = micro_count + section_count - 1

    def advance(moment, loop_state):
        arriving, collected = loop_state
        pick_index = jnp.clip(moment, 0, micro_count - 1)
        fresh_block = lax.dynamic_index_in_dim(fed_columns, pick_index, 0, keepdims=False)
        current = jnp.where(section_idx == 0, fresh_block, arriving)
        produced = mix_block(current)
        slot_index = moment - section_idx
        keep_flag = (
            (section_idx == section_count - 1) & (slot_index >= 0) & (slot_index < micro_count)
        )
        slot_safe = jnp.clip(slot_index, 0, micro_count - 1)
        previous = lax.dynamic_index_in_dim(collected, slot_safe, 0, keepdims=False)
        collected = lax.dynamic_update_index_in_dim(
            collected, jnp.where(keep_flag, produced, previous), slot_safe, 0
        )
        arriving = passed_along(produced, "pp", 1)
        return (arriving, collected)

    start_loop = (jnp.zeros_like(fed_columns[0]), jnp.zeros_like(fed_columns))
    arriving, collected = lax.fori_loop(0, total_steps, advance, start_loop)
    shared = from_root(collected, "pp", section_count - 1)
    token_share = length // section_count
    own_block = lax.dynamic_slice_in_dim(shared, section_idx * token_share, token_share, 2)
    as_float = own_block.astype(jnp.float32)
    partial_squares = jnp.sum(as_float * as_float, axis=1)
    total_squares = total_of_pieces(partial_squares, TP_FS)
    scale_rms = lax.rsqrt(total_squares / width_model + epsilon)
    result = (as_float * scale_rms[:, None, :]).astype(jnp.bfloat16)
    return jnp.swapaxes(result, 1, 2)


def solution(mesh):
    split = Mesh(
        mesh.devices.reshape(mesh.shape["pp"], mesh.shape["fs"], 4, 2), ("pp", "fs", "tp_0", "tp_1")
    )
    in_specs = (
        P(None, "pp", TP_FS),
        P("pp", None),
        P("pp", None, TP, "fs", None),
        P("pp", None, TP, "fs", None),
        P("pp", None, TP, None),
        P("pp", None, TP, None),
        P("pp", None, None, TP, "fs"),
        P("pp", None, TP, "fs"),
        P("pp", None, TP, "fs"),
        P("pp", TP, "fs"),
        P("pp", None, TP, "fs", None),
        P("pp", None, TP, None),
        P("pp", None, TP, None),
        P("pp", TP, "fs", None, None),
    )
    out_specs = P(None, "pp", TP_FS)
    return jax.shard_map(
        per_device, mesh=split, in_specs=in_specs, out_specs=out_specs, check_vma=False
    )
```

profile of v0, /device:TPU:1, one launch (start us, length us, event | category | flops | bytes accessed | tf_op | source)
XLA Modules:
  0.0 630.5 jit_solution(568530465908368264)
XLA Ops:
  6.5 1.1 copy.61
  8.7 2.2 concatenate.3
  11.0 10.3 %all_gather.25 = bf16[2,96,32]{2,0,1:T(2,128)(2,1)S(1)} all-gather(bf16[2,24,32]{2,0,1:T(2,128)(2,1)S(1)} %copy.60), channel_id=1, replica_groups=mesh['pp'=4,'fs'=4,'tp_0'=4,'tp_1'=2] {'pp'}, dimensions={1}, use_global_device_ids=true | all-gather | bytes 15360 | tf_op jit(solution)/shard_map/all_gather | solution.py:141
  22.8 547.7 %while.17 = (s32[]{:T(128)}, bf16[32,96]{1,0:T(8,128)(2,1)S(1)}, bf16[2,32,96]{2,1,0:T(8,128)(2,1)S(1)}, pred[]{:T(512)}, bf16[2,32,96]{2,1,0:T(8,128)(2,1)S(1)}...) while((s32[]{:T(128)}, bf16[32,96]{1,0:T(8,128)(2,1)S(1)}, ...), condition=%wide.region_7.8_spmd, body=%wide.region_0.7_spmd.sunk | while | flops 99476072 | bytes 4874331 | solution.py:232
  22.8 45.5 %all_gather.31 = bf16[1024,96]{1,0:T(8,128)(2,1)S(1)} all-gather(bf16[32,96]{1,0:T(8,128)(2,1)S(1)} %bitcast_select_fusion.3), channel_id=1, replica_groups=mesh['pp'=4,'fs'=4,'tp_0'=4,'tp_1'=2] {'tp_0','tp_1','fs'}, dimensions={0}, use_global_device_ids=true | all-gather | bytes 202752 | tf_op jit(solution)/shard_map/while/body/eval_jaxpr/all_gather | solution.py:162
  69.6 0.8 reverse_reduce_fusion.2
  71.0 0.9 fusion.75
  72.2 0.7 copy.77
  73.0 10.9 %reduce-scatter.4.cloned.1.call-done = bf16[16,32,96]{2,1,0:T(8,128)(2,1)} async-done(((bf16[32,32,96]{2,1,0:T(8,128)(2,1)}), bf16[16,32,96]{2,1,0:T(8,128)(2,1)}) %reduce-scatter.4.cloned.1.call-update) | async-done | bytes 98320 | tf_op jit(solution)/shard_map/while/body/eval_jaxpr/reduce_scatter | solution.py:18
  84.0 21.8 %reduce-scatter.6.cloned.1.call-done = bf16[4,32,96]{2,1,0:T(8,128)(2,1)} async-done(((bf16[16,32,96]{2,1,0:T(8,128)(2,1)}), bf16[4,32,96]{2,1,0:T(8,128)(2,1)}) %reduce-scatter.6.cloned.1.call-update) | async-done | bytes 24592 | tf_op jit(solution)/shard_map/while/body/eval_jaxpr/reduce_scatter | solution.py:18
  105.8 22.5 %reduce-scatter.8.cloned.1.call-done = bf16[1,32,96]{2,1,0:T(8,128)(2,1)} async-done(((bf16[4,32,96]{2,1,0:T(8,128)(2,1)}), bf16[1,32,96]{2,1,0:T(8,128)(2,1)}) %reduce-scatter.8.cloned.1.call-update) | async-done | bytes 6160 | tf_op jit(solution)/shard_map/while/body/eval_jaxpr/reduce_scatter | solution.py:18
  129.0 3.1 collective-permute-start
  132.2 0.8 collective-permute-done
  132.9 44.5 %all_gather.31 = bf16[1024,96]{1,0:T(8,128)(2,1)S(1)} all-gather(bf16[32,96]{1,0:T(8,128)(2,1)S(1)} %bitcast_select_fusion.3), channel_id=1, replica_groups=mesh['pp'=4,'fs'=4,'tp_0'=4,'tp_1'=2] {'tp_0','tp_1','fs'}, dimensions={0}, use_global_device_ids=true | all-gather | bytes 202752 | tf_op jit(solution)/shard_map/while/body/eval_jaxpr/all_gather | solution.py:162
  178.8 0.8 reverse_reduce_fusion.2
  180.2 0.9 fusion.75
  182.2 11.3 %reduce-scatter.4.cloned.1.call-done = bf16[16,32,96]{2,1,0:T(8,128)(2,1)} async-done(((bf16[32,32,96]{2,1,0:T(8,128)(2,1)}), bf16[16,32,96]{2,1,0:T(8,128)(2,1)}) %reduce-scatter.4.cloned.1.call-update) | async-done | bytes 98320 | tf_op jit(solution)/shard_map/while/body/eval_jaxpr/reduce_scatter | solution.py:18
  193.6 21.6 %reduce-scatter.6.cloned.1.call-done = bf16[4,32,96]{2,1,0:T(8,128)(2,1)} async-done(((bf16[16,32,96]{2,1,0:T(8,128)(2,1)}), bf16[4,32,96]{2,1,0:T(8,128)(2,1)}) %reduce-scatter.6.cloned.1.call-update) | async-done | bytes 24592 | tf_op jit(solution)/shard_map/while/body/eval_jaxpr/reduce_scatter | solution.py:18
  215.3 22.3 %reduce-scatter.8.cloned.1.call-done = bf16[1,32,96]{2,1,0:T(8,128)(2,1)} async-done(((bf16[4,32,96]{2,1,0:T(8,128)(2,1)}), bf16[1,32,96]{2,1,0:T(8,128)(2,1)}) %reduce-scatter.8.cloned.1.call-update) | async-done | bytes 6160 | tf_op jit(solution)/shard_map/while/body/eval_jaxpr/reduce_scatter | solution.py:18
  238.3 3.1 collective-permute-start
  241.4 0.8 collective-permute-done
  242.2 44.6 %all_gather.31 = bf16[1024,96]{1,0:T(8,128)(2,1)S(1)} all-gather(bf16[32,96]{1,0:T(8,128)(2,1)S(1)} %bitcast_select_fusion.3), channel_id=1, replica_groups=mesh['pp'=4,'fs'=4,'tp_0'=4,'tp_1'=2] {'tp_0','tp_1','fs'}, dimensions={0}, use_global_device_ids=true | all-gather | bytes 202752 | tf_op jit(solution)/shard_map/while/body/eval_jaxpr/all_gather | solution.py:162
  288.1 0.8 reverse_reduce_fusion.2
  289.5 0.9 fusion.75
  290.7 0.7 copy.77
  291.5 11.3 %reduce-scatter.4.cloned.1.call-done = bf16[16,32,96]{2,1,0:T(8,128)(2,1)} async-done(((bf16[32,32,96]{2,1,0:T(8,128)(2,1)}), bf16[16,32,96]{2,1,0:T(8,128)(2,1)}) %reduce-scatter.4.cloned.1.call-update) | async-done | bytes 98320 | tf_op jit(solution)/shard_map/while/body/eval_jaxpr/reduce_scatter | solution.py:18
  302.9 21.7 %reduce-scatter.6.cloned.1.call-done = bf16[4,32,96]{2,1,0:T(8,128)(2,1)} async-done(((bf16[16,32,96]{2,1,0:T(8,128)(2,1)}), bf16[4,32,96]{2,1,0:T(8,128)(2,1)}) %reduce-scatter.6.cloned.1.call-update) | async-done | bytes 24592 | tf_op jit(solution)/shard_map/while/body/eval_jaxpr/reduce_scatter | solution.py:18
  324.7 22.5 %reduce-scatter.8.cloned.1.call-done = bf16[1,32,96]{2,1,0:T(8,128)(2,1)} async-done(((bf16[4,32,96]{2,1,0:T(8,128)(2,1)}), bf16[1,32,96]{2,1,0:T(8,128)(2,1)}) %reduce-scatter.8.cloned.1.call-update) | async-done | bytes 6160 | tf_op jit(solution)/shard_map/while/body/eval_jaxpr/reduce_scatter | solution.py:18
  347.9 3.1 collective-permute-start
  351.0 0.8 collective-permute-done
  351.8 44.5 %all_gather.31 = bf16[1024,96]{1,0:T(8,128)(2,1)S(1)} all-gather(bf16[32,96]{1,0:T(8,128)(2,1)S(1)} %bitcast_select_fusion.3), channel_id=1, replica_groups=mesh['pp'=4,'fs'=4,'tp_0'=4,'tp_1'=2] {'tp_0','tp_1','fs'}, dimensions={0}, use_global_device_ids=true | all-gather | bytes 202752 | tf_op jit(solution)/shard_map/while/body/eval_jaxpr/all_gather | solution.py:162
  397.6 0.8 reverse_reduce_fusion.2
  399.0 0.9 fusion.75
  401.1 11.4 %reduce-scatter.4.cloned.1.call-done = bf16[16,32,96]{2,1,0:T(8,128)(2,1)} async-done(((bf16[32,32,96]{2,1,0:T(8,128)(2,1)}), bf16[16,32,96]{2,1,0:T(8,128)(2,1)}) %reduce-scatter.4.cloned.1.call-update) | async-done | bytes 98320 | tf_op jit(solution)/shard_map/while/body/eval_jaxpr/reduce_scatter | solution.py:18
  412.5 21.7 %reduce-scatter.6.cloned.1.call-done = bf16[4,32,96]{2,1,0:T(8,128)(2,1)} async-done(((bf16[16,32,96]{2,1,0:T(8,128)(2,1)}), bf16[4,32,96]{2,1,0:T(8,128)(2,1)}) %reduce-scatter.6.cloned.1.call-update) | async-done | bytes 24592 | tf_op jit(solution)/shard_map/while/body/eval_jaxpr/reduce_scatter | solution.py:18
  434.3 22.3 %reduce-scatter.8.cloned.1.call-done = bf16[1,32,96]{2,1,0:T(8,128)(2,1)} async-done(((bf16[4,32,96]{2,1,0:T(8,128)(2,1)}), bf16[1,32,96]{2,1,0:T(8,128)(2,1)}) %reduce-scatter.8.cloned.1.call-update) | async-done | bytes 6160 | tf_op jit(solution)/shard_map/while/body/eval_jaxpr/reduce_scatter | solution.py:18
  457.3 3.1 collective-permute-start
  460.4 0.8 collective-permute-done
  461.2 44.6 %all_gather.31 = bf16[1024,96]{1,0:T(8,128)(2,1)S(1)} all-gather(bf16[32,96]{1,0:T(8,128)(2,1)S(1)} %bitcast_select_fusion.3), channel_id=1, replica_groups=mesh['pp'=4,'fs'=4,'tp_0'=4,'tp_1'=2] {'tp_0','tp_1','fs'}, dimensions={0}, use_global_device_ids=true | all-gather | bytes 202752 | tf_op jit(solution)/shard_map/while/body/eval_jaxpr/all_gather | solution.py:162
  507.1 0.8 reverse_reduce_fusion.2
  508.5 0.9 fusion.75
  510.5 11.3 %reduce-scatter.4.cloned.1.call-done = bf16[16,32,96]{2,1,0:T(8,128)(2,1)} async-done(((bf16[32,32,96]{2,1,0:T(8,128)(2,1)}), bf16[16,32,96]{2,1,0:T(8,128)(2,1)}) %reduce-scatter.4.cloned.1.call-update) | async-done | bytes 98320 | tf_op jit(solution)/shard_map/while/body/eval_jaxpr/reduce_scatter | solution.py:18
  521.9 21.6 %reduce-scatter.6.cloned.1.call-done = bf16[4,32,96]{2,1,0:T(8,128)(2,1)} async-done(((bf16[16,32,96]{2,1,0:T(8,128)(2,1)}), bf16[4,32,96]{2,1,0:T(8,128)(2,1)}) %reduce-scatter.6.cloned.1.call-update) | async-done | bytes 24592 | tf_op jit(solution)/shard_map/while/body/eval_jaxpr/reduce_scatter | solution.py:18
  543.6 22.3 %reduce-scatter.8.cloned.1.call-done = bf16[1,32,96]{2,1,0:T(8,128)(2,1)} async-done(((bf16[4,32,96]{2,1,0:T(8,128)(2,1)}), bf16[1,32,96]{2,1,0:T(8,128)(2,1)}) %reduce-scatter.8.cloned.1.call-update) | async-done | bytes 6160 | tf_op jit(solution)/shard_map/while/body/eval_jaxpr/reduce_scatter | solution.py:18
  566.6 3.1 collective-permute-start
  569.7 0.8 collective-permute-done
  570.5 10.1 %all-gather = bf16[8,32,96]{2,1,0:T(8,128)(2,1)S(1)} all-gather(bf16[2,32,96]{2,1,0:T(8,128)(2,1)S(1)} %get-tuple-element.349), channel_id=2, replica_groups=mesh['pp'=4,'fs'=4,'tp_0'=4,'tp_1'=2] {'pp'}, dimensions={0}, use_global_device_ids=true | all-gather | bytes 61440 | tf_op jit(solution)/shard_map/all_gather | solution.py:45
  580.7 42.5 %all-gather.2 = f32[32,2,24]{2,1,0:T(2,128)S(1)} all-gather(f32[1,2,24]{2,1,0:T(2,128)S(1)} %bitcast.173), channel_id=3, replica_groups=mesh['pp'=4,'fs'=4,'tp_0'=4,'tp_1'=2] {'tp_0','tp_1','fs'}, dimensions={0}, use_global_device_ids=true | all-gather | bytes 6336 | tf_op jit(solution)/shard_map/all_gather | solution.py:49
  (190 shorter events, 20.9 us)
Async XLA Ops:
  6.5 1.1 copy-start.3
  6.5 1.3 copy-start.10
  7.7 1.0 copy-start.1
  7.7 1.0 copy-start.2
  8.7 2.2 copy-start.9
  10.9 11.2 %copy-start = (bf16[1,1,1,64,1024]{4,3,2,1,0:T(8,128)(2,1)S(1)}, bf16[1,1,1,64,1024]{4,3,2,1,0:T(8,128)(2,1)}, u32[]{:S(2)}) copy-start(bf16[1,1,1,64,1024]{4,3,2,1,0:T(8,128)(2,1)} %param.29) | copy-start | bytes 393220
  21.3 0.8 copy-start.6
  21.3 0.8 copy-start.7
  21.4 0.7 copy-start.11
  22.0 0.7 copy-start.4
  22.1 0.7 copy-start.5
  22.1 0.7 copy-start.8
  22.8 61.2 %reduce-scatter.4.cloned.1.call-start = ((), (), s32[]{:S(2)}) async-start(), calls=%async_computation.3 | async-start | bytes 393216 | tf_op jit(solution)/shard_map/while/body/eval_jaxpr/reduce_scatter | solution.py:18
  73.0 32.8 %reduce-scatter.6.cloned.1.call-start = ((), (), s32[]{:S(2)}) async-start(), calls=%async_computation.4 | async-start | bytes 163840 | tf_op jit(solution)/shard_map/while/body/eval_jaxpr/reduce_scatter | solution.py:18
  84.0 44.4 %reduce-scatter.8.cloned.1.call-start = ((), (), s32[]{:S(2)}) async-start(), calls=%async_computation.5 | async-start | bytes 40960 | tf_op jit(solution)/shard_map/while/body/eval_jaxpr/reduce_scatter | solution.py:18
  129.0 3.9 collective-permute-start
  132.9 60.6 %reduce-scatter.4.cloned.1.call-start = ((), (), s32[]{:S(2)}) async-start(), calls=%async_computation.3 | async-start | bytes 393216 | tf_op jit(solution)/shard_map/while/body/eval_jaxpr/reduce_scatter | solution.py:18
  182.2 33.0 %reduce-scatter.6.cloned.1.call-start = ((), (), s32[]{:S(2)}) async-start(), calls=%async_computation.4 | async-start | bytes 163840 | tf_op jit(solution)/shard_map/while/body/eval_jaxpr/reduce_scatter | solution.py:18
  193.6 44.0 %reduce-scatter.8.cloned.1.call-start = ((), (), s32[]{:S(2)}) async-start(), calls=%async_computation.5 | async-start | bytes 40960 | tf_op jit(solution)/shard_map/while/body/eval_jaxpr/reduce_scatter | solution.py:18
  238.3 3.9 collective-permute-start
  242.2 60.7 %reduce-scatter.4.cloned.1.call-start = ((), (), s32[]{:S(2)}) async-start(), calls=%async_computation.3 | async-start | bytes 393216 | tf_op jit(solution)/shard_map/while/body/eval_jaxpr/reduce_scatter | solution.py:18
  291.5 33.2 %reduce-scatter.6.cloned.1.call-start = ((), (), s32[]{:S(2)}) async-start(), calls=%async_computation.4 | async-start | bytes 163840 | tf_op jit(solution)/shard_map/while/body/eval_jaxpr/reduce_scatter | solution.py:18
  302.9 44.3 %reduce-scatter.8.cloned.1.call-start = ((), (), s32[]{:S(2)}) async-start(), calls=%async_computation.5 | async-start | bytes 40960 | tf_op jit(solution)/shard_map/while/body/eval_jaxpr/reduce_scatter | solution.py:18
  347.9 3.9 collective-permute-start
  351.7 60.7 %reduce-scatter.4.cloned.1.call-start = ((), (), s32[]{:S(2)}) async-start(), calls=%async_computation.3 | async-start | bytes 393216 | tf_op jit(solution)/shard_map/while/body/eval_jaxpr/reduce_scatter | solution.py:18
  401.0 33.2 %reduce-scatter.6.cloned.1.call-start = ((), (), s32[]{:S(2)}) async-start(), calls=%async_computation.4 | async-start | bytes 163840 | tf_op jit(solution)/shard_map/while/body/eval_jaxpr/reduce_scatter | solution.py:18
  412.5 44.2 %reduce-scatter.8.cloned.1.call-start = ((), (), s32[]{:S(2)}) async-start(), calls=%async_computation.5 | async-start | bytes 40960 | tf_op jit(solution)/shard_map/while/body/eval_jaxpr/reduce_scatter | solution.py:18
  457.3 3.8 collective-permute-start
  461.2 60.7 %reduce-scatter.4.cloned.1.call-start = ((), (), s32[]{:S(2)}) async-start(), calls=%async_computation.3 | async-start | bytes 393216 | tf_op jit(solution)/shard_map/while/body/eval_jaxpr/reduce_scatter | solution.py:18
  510.5 33.1 %reduce-scatter.6.cloned.1.call-start = ((), (), s32[]{:S(2)}) async-start(), calls=%async_computation.4 | async-start | bytes 163840 | tf_op jit(solution)/shard_map/while/body/eval_jaxpr/reduce_scatter | solution.py:18
  521.9 44.0 %reduce-scatter.8.cloned.1.call-start = ((), (), s32[]{:S(2)}) async-start(), calls=%async_computation.5 | async-start | bytes 40960 | tf_op jit(solution)/shard_map/while/body/eval_jaxpr/reduce_scatter | solution.py:18
  566.6 3.9 collective-permute-start
Sparse Core Ops, SparseCore 0:
  73.1 10.8 reduce-scatter.3
  86.3 19.4 reduce-scatter.5
  108.1 20.1 reduce-scatter.7
  182.3 11.2 reduce-scatter.3
  195.8 19.4 reduce-scatter.5
  217.4 20.0 reduce-scatter.7
  291.6 11.2 reduce-scatter.3
  305.2 19.4 reduce-scatter.5
  327.0 20.1 reduce-scatter.7
  401.1 11.2 reduce-scatter.3
  414.8 19.4 reduce-scatter.5
  436.4 20.1 reduce-scatter.7
  510.6 11.2 reduce-scatter.3
  524.1 19.4 reduce-scatter.5
  545.7 20.1 reduce-scatter.7
where the time goes:
time: 631 us; the launch traced here: 630 us
  blocking collectives  287 us (45%)
  waiting for transfers between devices  281 us (45%)
  local copies, waits for them, and re-layouts  16.9 us (3%)
  starting transfers between devices  15.9 us (3%)
  between operations  13.2 us (2%)
  matrix products  9.24 us (1%)
  other arithmetic  7.19 us (1%)
    reduce_scatter x15, waiting for transfers between devices, sum_in_order(): parts = lax.psum_scatter(parts, axes[k], scatter_dimension=0, tiled=True)  277 us
    all_gather x5, blocking collectives, project(): gathered = lax.all_gather(column_block, TP_FS, axis=0, tiled=True)  224 us
    all_gather x1, blocking collectives, total_of_pieces(): return lax.all_gather(shard, axis).sum(0)  42.5 us
    ppermute x5, starting transfers between devices, passed_along(): return lax.ppermute(shard, axis, pairs)  15.4 us
  transfers between devices with their start and end apart: 20, of which 20 were waited for; matrix products, arithmetic and copies ran while one was open for 0% of the time, Pallas kernels for 0%

commit v1 on v0

--- a/solution.py
+++ b/solution.py
@@ -159,7 +159,9 @@
     own_rows = width_model // lax.axis_size(TP_FS)
 
     def project(column_block):
-        gathered = lax.all_gather(column_block, TP_FS, axis=0, tiled=True)
+        r_now = jnp.stack(lax.axis_size(TP_FS) * [column_block])
+        r2 = lax.all_to_all(r_now, axis_name=TP_FS, split_axis=0, concat_axis=0)
+        gathered = jnp.concatenate(r2, 0)
         as_float = gathered.astype(jnp.float32)
         scale_rms = lax.rsqrt(jnp.mean(as_float * as_float, axis=0) + epsilon)
         normed = (as_float * scale_rms[None, :] * gain_vec[:, None]).astype(jnp.bfloat16)

time: 631 us -> 494 us (0.78)
  blocking collectives: 287 us -> 62.8 us
  starting transfers between devices: 15.9 us -> 65 us
  waiting for transfers between devices: 281 us -> 314 us
    all_gather x5 -> x0, blocking collectives: 224 us -> none  [project(): gathered = lax.all_gather(column_block, TP_FS, axis=0, tiled=True)]
    all_to_all x0 -> x5, starting transfers between devices: none -> 48.9 us  [project(): r2 = lax.all_to_all(r_now, axis_name=TP_FS, split_axis=0, concat_axis=0)]
    all_to_all x0 -> x5, waiting for transfers between devices: none -> 44 us  [project(): r2 = lax.all_to_all(r_now, axis_name=TP_FS, split_axis=0, concat_axis=0)]
    reduce_scatter x15, waiting for transfers between devices: 277 us -> 266 us  [sum_in_order(): parts = lax.psum_scatter(parts, axes[k], scatter_dimension=0, tiled=True)]
  transfers between devices with their start and end apart: 20 -> 25, of which waited for: 20 -> 25; matrix products, arithmetic and copies ran while one was open for 0% -> 0% of each run, Pallas kernels for 0% -> 0%
where the time goes in v1:
time: 494 us; the launch traced here: 493 us
  waiting for transfers between devices  314 us (64%)
  starting transfers between devices  65 us (13%)
  blocking collectives  62.8 us (13%)
  local copies, waits for them, and re-layouts  20.6 us (4%)
  between operations  13.2 us (3%)
  other arithmetic  8.23 us (2%)
  matrix products  8.09 us (2%)
    reduce_scatter x15, waiting for transfers between devices, sum_in_order(): parts = lax.psum_scatter(parts, axes[k], scatter_dimension=0, tiled=True)  266 us
    all_to_all x5, starting transfers between devices, project(): r2 = lax.all_to_all(r_now, axis_name=TP_FS, split_axis=0, concat_axis=0)  48.9 us
    all_to_all x5, waiting for transfers between devices, project(): r2 = lax.all_to_all(r_now, axis_name=TP_FS, split_axis=0, concat_axis=0)  44 us
    all_gather x1, blocking collectives, total_of_pieces(): return lax.all_gather(shard, axis).sum(0)  42.5 us
    ppermute x5, starting transfers between devices, passed_along(): return lax.ppermute(shard, axis, pairs)  15.5 us
    all_gather x1, blocking collectives, per_device(): fed_blocks = lax.all_gather(micro_in, 'pp', axis=1, tiled=True)  10.3 us
    all_gather x1, blocking collectives, from_root(): lax.all_gather(shard, axis)  10 us
  transfers between devices with their start and end apart: 25, of which 25 were waited for; matrix products, arithmetic and copies ran while one was open for 0% of the time, Pallas kernels for 0%

profile of v1, /device:TPU:1, one launch (start us, length us, event | category | flops | bytes accessed | tf_op | source)
XLA Modules:
  0.0 493.3 jit_solution(6209931284737676635)
XLA Ops:
  6.5 1.1 copy.72
  8.7 2.2 concatenate.3
  11.0 10.3 %all_gather.15 = bf16[2,96,32]{2,0,1:T(2,128)(2,1)S(1)} all-gather(bf16[2,24,32]{2,0,1:T(2,128)(2,1)S(1)} %copy.71), channel_id=1, replica_groups=mesh['pp'=4,'fs'=4,'tp_0'=4,'tp_1'=2] {'pp'}, dimensions={1}, use_global_device_ids=true | all-gather | bytes 15360 | tf_op jit(solution)/shard_map/all_gather | solution.py:141
  22.8 410.6 %while.17 = (s32[]{:T(128)}, bf16[32,96]{1,0:T(8,128)(2,1)S(1)}, bf16[2,32,96]{2,1,0:T(8,128)(2,1)S(1)}, pred[]{:T(512)}, bf16[2,32,96]{2,1,0:T(8,128)(2,1)S(1)}...) while((s32[]{:T(128)}, bf16[32,96]{1,0:T(8,128)(2,1)S(1)}, ...), condition=%wide.region_7.8_spmd, body=%wide.region_0.7_spmd.sunk | while | flops 99476072 | bytes 5988475 | solution.py:234
  23.5 11.7 %all-to-all-start = ((bf16[32,32,96]{2,1,0:T(8,128)(2,1)}), bf16[32,32,96]{2,1,0:T(8,128)(2,1)S(1)}, u32[]{:S(2)}, u32[]{:S(2)}) async-start(bf16[32,32,96]{2,1,0:T(8,128)(2,1)} %stack.7), calls=%async_computation | async-start | bytes 524288 | tf_op jit(solution)/shard_map/while/body/eval_jaxpr/all_to_all | solution.py:163
  35.2 8.8 %all-to-all-done = bf16[32,32,96]{2,1,0:T(8,128)(2,1)S(1)} async-done(((bf16[32,32,96]{2,1,0:T(8,128)(2,1)}), bf16[32,32,96]{2,1,0:T(8,128)(2,1)S(1)}, u32[]{:S(2)}, u32[]{:S(2)}) %all-to-all-start) | async-done | bytes 196640 | tf_op jit(solution)/shard_map/while/body/eval_jaxpr/all_to_all | solution.py:163
  45.3 0.8 reverse_reduce_fusion.2
  46.7 0.9 fusion.73
  48.8 8.1 %reduce-scatter.4.cloned.1.call-done = bf16[16,32,96]{2,1,0:T(8,128)(2,1)} async-done(((bf16[32,32,96]{2,1,0:T(8,128)(2,1)}), bf16[16,32,96]{2,1,0:T(8,128)(2,1)}) %reduce-scatter.4.cloned.1.call-update) | async-done | bytes 98320 | tf_op jit(solution)/shard_map/while/body/eval_jaxpr/reduce_scatter | solution.py:18
  56.9 21.7 %reduce-scatter.6.cloned.1.call-done = bf16[4,32,96]{2,1,0:T(8,128)(2,1)} async-done(((bf16[16,32,96]{2,1,0:T(8,128)(2,1)}), bf16[4,32,96]{2,1,0:T(8,128)(2,1)}) %reduce-scatter.6.cloned.1.call-update) | async-done | bytes 24592 | tf_op jit(solution)/shard_map/while/body/eval_jaxpr/reduce_scatter | solution.py:18
  78.7 22.5 %reduce-scatter.8.cloned.1.call-done = bf16[1,32,96]{2,1,0:T(8,128)(2,1)} async-done(((bf16[4,32,96]{2,1,0:T(8,128)(2,1)}), bf16[1,32,96]{2,1,0:T(8,128)(2,1)}) %reduce-scatter.8.cloned.1.call-update) | async-done | bytes 6160 | tf_op jit(solution)/shard_map/while/body/eval_jaxpr/reduce_scatter | solution.py:18
  101.9 3.1 collective-permute-start
  105.1 0.8 collective-permute-done
  106.6 9.3 %all-to-all-start = ((bf16[32,32,96]{2,1,0:T(8,128)(2,1)}), bf16[32,32,96]{2,1,0:T(8,128)(2,1)S(1)}, u32[]{:S(2)}, u32[]{:S(2)}) async-start(bf16[32,32,96]{2,1,0:T(8,128)(2,1)} %stack.7), calls=%async_computation | async-start | bytes 524288 | tf_op jit(solution)/shard_map/while/body/eval_jaxpr/all_to_all | solution.py:163
  116.0 8.8 %all-to-all-done = bf16[32,32,96]{2,1,0:T(8,128)(2,1)S(1)} async-done(((bf16[32,32,96]{2,1,0:T(8,128)(2,1)}), bf16[32,32,96]{2,1,0:T(8,128)(2,1)S(1)}, u32[]{:S(2)}, u32[]{:S(2)}) %all-to-all-start) | async-done | bytes 196640 | tf_op jit(solution)/shard_map/while/body/eval_jaxpr/all_to_all | solution.py:163
  126.1 0.8 reverse_reduce_fusion.2
  127.4 0.9 fusion.73
  129.5 9.5 %reduce-scatter.4.cloned.1.call-done = bf16[16,32,96]{2,1,0:T(8,128)(2,1)} async-done(((bf16[32,32,96]{2,1,0:T(8,128)(2,1)}), bf16[16,32,96]{2,1,0:T(8,128)(2,1)}) %reduce-scatter.4.cloned.1.call-update) | async-done | bytes 98320 | tf_op jit(solution)/shard_map/while/body/eval_jaxpr/reduce_scatter | solution.py:18
  139.0 21.6 %reduce-scatter.6.cloned.1.call-done = bf16[4,32,96]{2,1,0:T(8,128)(2,1)} async-done(((bf16[16,32,96]{2,1,0:T(8,128)(2,1)}), bf16[4,32,96]{2,1,0:T(8,128)(2,1)}) %reduce-scatter.6.cloned.1.call-update) | async-done | bytes 24592 | tf_op jit(solution)/shard_map/while/body/eval_jaxpr/reduce_scatter | solution.py:18
  160.7 22.3 %reduce-scatter.8.cloned.1.call-done = bf16[1,32,96]{2,1,0:T(8,128)(2,1)} async-done(((bf16[4,32,96]{2,1,0:T(8,128)(2,1)}), bf16[1,32,96]{2,1,0:T(8,128)(2,1)}) %reduce-scatter.8.cloned.1.call-update) | async-done | bytes 6160 | tf_op jit(solution)/shard_map/while/body/eval_jaxpr/reduce_scatter | solution.py:18
  183.7 3.1 collective-permute-start
  186.8 0.8 collective-permute-done
  188.3 9.3 %all-to-all-start = ((bf16[32,32,96]{2,1,0:T(8,128)(2,1)}), bf16[32,32,96]{2,1,0:T(8,128)(2,1)S(1)}, u32[]{:S(2)}, u32[]{:S(2)}) async-start(bf16[32,32,96]{2,1,0:T(8,128)(2,1)} %stack.7), calls=%async_computation | async-start | bytes 524288 | tf_op jit(solution)/shard_map/while/body/eval_jaxpr/all_to_all | solution.py:163
  197.7 8.8 %all-to-all-done = bf16[32,32,96]{2,1,0:T(8,128)(2,1)S(1)} async-done(((bf16[32,32,96]{2,1,0:T(8,128)(2,1)}), bf16[32,32,96]{2,1,0:T(8,128)(2,1)S(1)}, u32[]{:S(2)}, u32[]{:S(2)}) %all-to-all-start) | async-done | bytes 196640 | tf_op jit(solution)/shard_map/while/body/eval_jaxpr/all_to_all | solution.py:163
  207.8 0.8 reverse_reduce_fusion.2
  209.2 0.9 fusion.73
  211.2 9.5 %reduce-scatter.4.cloned.1.call-done = bf16[16,32,96]{2,1,0:T(8,128)(2,1)} async-done(((bf16[32,32,96]{2,1,0:T(8,128)(2,1)}), bf16[16,32,96]{2,1,0:T(8,128)(2,1)}) %reduce-scatter.4.cloned.1.call-update) | async-done | bytes 98320 | tf_op jit(solution)/shard_map/while/body/eval_jaxpr/reduce_scatter | solution.py:18
  220.8 21.8 %reduce-scatter.6.cloned.1.call-done = bf16[4,32,96]{2,1,0:T(8,128)(2,1)} async-done(((bf16[16,32,96]{2,1,0:T(8,128)(2,1)}), bf16[4,32,96]{2,1,0:T(8,128)(2,1)}) %reduce-scatter.6.cloned.1.call-update) | async-done | bytes 24592 | tf_op jit(solution)/shard_map/while/body/eval_jaxpr/reduce_scatter | solution.py:18
  242.6 22.5 %reduce-scatter.8.cloned.1.call-done = bf16[1,32,96]{2,1,0:T(8,128)(2,1)} async-done(((bf16[4,32,96]{2,1,0:T(8,128)(2,1)}), bf16[1,32,96]{2,1,0:T(8,128)(2,1)}) %reduce-scatter.8.cloned.1.call-update) | async-done | bytes 6160 | tf_op jit(solution)/shard_map/while/body/eval_jaxpr/reduce_scatter | solution.py:18
  265.8 3.1 collective-permute-start
  270.4 9.3 %all-to-all-start = ((bf16[32,32,96]{2,1,0:T(8,128)(2,1)}), bf16[32,32,96]{2,1,0:T(8,128)(2,1)S(1)}, u32[]{:S(2)}, u32[]{:S(2)}) async-start(bf16[32,32,96]{2,1,0:T(8,128)(2,1)} %stack.7), calls=%async_computation | async-start | bytes 524288 | tf_op jit(solution)/shard_map/while/body/eval_jaxpr/all_to_all | solution.py:163
  279.8 8.8 %all-to-all-done = bf16[32,32,96]{2,1,0:T(8,128)(2,1)S(1)} async-done(((bf16[32,32,96]{2,1,0:T(8,128)(2,1)}), bf16[32,32,96]{2,1,0:T(8,128)(2,1)S(1)}, u32[]{:S(2)}, u32[]{:S(2)}) %all-to-all-start) | async-done | bytes 196640 | tf_op jit(solution)/shard_map/while/body/eval_jaxpr/all_to_all | solution.py:163
  289.9 0.8 reverse_reduce_fusion.2
  291.3 0.9 fusion.73
  293.3 9.5 %reduce-scatter.4.cloned.1.call-done = bf16[16,32,96]{2,1,0:T(8,128)(2,1)} async-done(((bf16[32,32,96]{2,1,0:T(8,128)(2,1)}), bf16[16,32,96]{2,1,0:T(8,128)(2,1)}) %reduce-scatter.4.cloned.1.call-update) | async-done | bytes 98320 | tf_op jit(solution)/shard_map/while/body/eval_jaxpr/reduce_scatter | solution.py:18
  302.9 21.7 %reduce-scatter.6.cloned.1.call-done = bf16[4,32,96]{2,1,0:T(8,128)(2,1)} async-done(((bf16[16,32,96]{2,1,0:T(8,128)(2,1)}), bf16[4,32,96]{2,1,0:T(8,128)(2,1)}) %reduce-scatter.6.cloned.1.call-update) | async-done | bytes 24592 | tf_op jit(solution)/shard_map/while/body/eval_jaxpr/reduce_scatter | solution.py:18
  324.7 22.3 %reduce-scatter.8.cloned.1.call-done = bf16[1,32,96]{2,1,0:T(8,128)(2,1)} async-done(((bf16[4,32,96]{2,1,0:T(8,128)(2,1)}), bf16[1,32,96]{2,1,0:T(8,128)(2,1)}) %reduce-scatter.8.cloned.1.call-update) | async-done | bytes 6160 | tf_op jit(solution)/shard_map/while/body/eval_jaxpr/reduce_scatter | solution.py:18
  347.7 3.1 collective-permute-start
  352.3 9.3 %all-to-all-start = ((bf16[32,32,96]{2,1,0:T(8,128)(2,1)}), bf16[32,32,96]{2,1,0:T(8,128)(2,1)S(1)}, u32[]{:S(2)}, u32[]{:S(2)}) async-start(bf16[32,32,96]{2,1,0:T(8,128)(2,1)} %stack.7), calls=%async_computation | async-start | bytes 524288 | tf_op jit(solution)/shard_map/while/body/eval_jaxpr/all_to_all | solution.py:163
  361.7 8.8 %all-to-all-done = bf16[32,32,96]{2,1,0:T(8,128)(2,1)S(1)} async-done(((bf16[32,32,96]{2,1,0:T(8,128)(2,1)}), bf16[32,32,96]{2,1,0:T(8,128)(2,1)S(1)}, u32[]{:S(2)}, u32[]{:S(2)}) %all-to-all-start) | async-done | bytes 196640 | tf_op jit(solution)/shard_map/while/body/eval_jaxpr/all_to_all | solution.py:163
  371.8 0.8 reverse_reduce_fusion.2
  373.2 0.9 fusion.73
  375.2 9.5 %reduce-scatter.4.cloned.1.call-done = bf16[16,32,96]{2,1,0:T(8,128)(2,1)} async-done(((bf16[32,32,96]{2,1,0:T(8,128)(2,1)}), bf16[16,32,96]{2,1,0:T(8,128)(2,1)}) %reduce-scatter.4.cloned.1.call-update) | async-done | bytes 98320 | tf_op jit(solution)/shard_map/while/body/eval_jaxpr/reduce_scatter | solution.py:18
  384.8 21.6 %reduce-scatter.6.cloned.1.call-done = bf16[4,32,96]{2,1,0:T(8,128)(2,1)} async-done(((bf16[16,32,96]{2,1,0:T(8,128)(2,1)}), bf16[4,32,96]{2,1,0:T(8,128)(2,1)}) %reduce-scatter.6.cloned.1.call-update) | async-done | bytes 24592 | tf_op jit(solution)/shard_map/while/body/eval_jaxpr/reduce_scatter | solution.py:18
  406.4 22.3 %reduce-scatter.8.cloned.1.call-done = bf16[1,32,96]{2,1,0:T(8,128)(2,1)} async-done(((bf16[4,32,96]{2,1,0:T(8,128)(2,1)}), bf16[1,32,96]{2,1,0:T(8,128)(2,1)}) %reduce-scatter.8.cloned.1.call-update) | async-done | bytes 6160 | tf_op jit(solution)/shard_map/while/body/eval_jaxpr/reduce_scatter | solution.py:18
  429.4 3.1 collective-permute-start
  433.3 10.0 %all-gather = bf16[8,32,96]{2,1,0:T(8,128)(2,1)S(1)} all-gather(bf16[2,32,96]{2,1,0:T(8,128)(2,1)S(1)} %get-tuple-element.349), channel_id=2, replica_groups=mesh['pp'=4,'fs'=4,'tp_0'=4,'tp_1'=2] {'pp'}, dimensions={0}, use_global_device_ids=true | all-gather | bytes 61440 | tf_op jit(solution)/shard_map/all_gather | solution.py:45
  443.5 42.5 %all-gather.2 = f32[32,2,24]{2,1,0:T(2,128)S(1)} all-gather(f32[1,2,24]{2,1,0:T(2,128)S(1)} %bitcast.184), channel_id=3, replica_groups=mesh['pp'=4,'fs'=4,'tp_0'=4,'tp_1'=2] {'tp_0','tp_1','fs'}, dimensions={0}, use_global_device_ids=true | all-gather | bytes 6336 | tf_op jit(solution)/shard_map/all_gather | solution.py:49
  (205 shorter events, 28.4 us)
Async XLA Ops:
  6.5 1.1 copy-start.3
  6.5 1.3 copy-start.10
  7.7 1.0 copy-start.1
  7.7 1.0 copy-start.2
  8.7 2.2 copy-start.9
  10.9 11.2 %copy-start = (bf16[1,1,1,64,1024]{4,3,2,1,0:T(8,128)(2,1)S(1)}, bf16[1,1,1,64,1024]{4,3,2,1,0:T(8,128)(2,1)}, u32[]{:S(2)}) copy-start(bf16[1,1,1,64,1024]{4,3,2,1,0:T(8,128)(2,1)} %param.29) | copy-start | bytes 393220
  21.3 0.8 copy-start.6
  21.3 0.8 copy-start.7
  21.4 0.7 copy-start.11
  22.0 0.7 copy-start.4
  22.1 0.7 copy-start.5
  22.1 0.7 copy-start.8
  23.5 20.5 %all-to-all-start = ((bf16[32,32,96]{2,1,0:T(8,128)(2,1)}), bf16[32,32,96]{2,1,0:T(8,128)(2,1)S(1)}, u32[]{:S(2)}, u32[]{:S(2)}) async-start(bf16[32,32,96]{2,1,0:T(8,128)(2,1)} %stack.7), calls=%async_computation | async-start | bytes 524288 | tf_op jit(solution)/shard_map/while/body/eval_jaxpr/all_to_all | solution.py:163
  35.2 21.7 %reduce-scatter.4.cloned.1.call-start = ((), (), s32[]{:S(2)}) async-start(), calls=%async_computation.4 | async-start | bytes 393216 | tf_op jit(solution)/shard_map/while/body/eval_jaxpr/reduce_scatter | solution.py:18
  48.7 29.9 %reduce-scatter.6.cloned.1.call-start = ((), (), s32[]{:S(2)}) async-start(), calls=%async_computation.5 | async-start | bytes 163840 | tf_op jit(solution)/shard_map/while/body/eval_jaxpr/reduce_scatter | solution.py:18
  56.9 44.3 %reduce-scatter.8.cloned.1.call-start = ((), (), s32[]{:S(2)}) async-start(), calls=%async_computation.6 | async-start | bytes 40960 | tf_op jit(solution)/shard_map/while/body/eval_jaxpr/reduce_scatter | solution.py:18
  101.9 3.9 collective-permute-start
  106.6 18.2 %all-to-all-start = ((bf16[32,32,96]{2,1,0:T(8,128)(2,1)}), bf16[32,32,96]{2,1,0:T(8,128)(2,1)S(1)}, u32[]{:S(2)}, u32[]{:S(2)}) async-start(bf16[32,32,96]{2,1,0:T(8,128)(2,1)} %stack.7), calls=%async_computation | async-start | bytes 524288 | tf_op jit(solution)/shard_map/while/body/eval_jaxpr/all_to_all | solution.py:163
  115.9 23.1 %reduce-scatter.4.cloned.1.call-start = ((), (), s32[]{:S(2)}) async-start(), calls=%async_computation.4 | async-start | bytes 393216 | tf_op jit(solution)/shard_map/while/body/eval_jaxpr/reduce_scatter | solution.py:18
  129.4 31.2 %reduce-scatter.6.cloned.1.call-start = ((), (), s32[]{:S(2)}) async-start(), calls=%async_computation.5 | async-start | bytes 163840 | tf_op jit(solution)/shard_map/while/body/eval_jaxpr/reduce_scatter | solution.py:18
  139.0 44.0 %reduce-scatter.8.cloned.1.call-start = ((), (), s32[]{:S(2)}) async-start(), calls=%async_computation.6 | async-start | bytes 40960 | tf_op jit(solution)/shard_map/while/body/eval_jaxpr/reduce_scatter | solution.py:18
  183.7 3.9 collective-permute-start
  188.3 18.2 %all-to-all-start = ((bf16[32,32,96]{2,1,0:T(8,128)(2,1)}), bf16[32,32,96]{2,1,0:T(8,128)(2,1)S(1)}, u32[]{:S(2)}, u32[]{:S(2)}) async-start(bf16[32,32,96]{2,1,0:T(8,128)(2,1)} %stack.7), calls=%async_computation | async-start | bytes 524288 | tf_op jit(solution)/shard_map/while/body/eval_jaxpr/all_to_all | solution.py:163
  197.6 23.1 %reduce-scatter.4.cloned.1.call-start = ((), (), s32[]{:S(2)}) async-start(), calls=%async_computation.4 | async-start | bytes 393216 | tf_op jit(solution)/shard_map/while/body/eval_jaxpr/reduce_scatter | solution.py:18
  211.2 31.4 %reduce-scatter.6.cloned.1.call-start = ((), (), s32[]{:S(2)}) async-start(), calls=%async_computation.5 | async-start | bytes 163840 | tf_op jit(solution)/shard_map/while/body/eval_jaxpr/reduce_scatter | solution.py:18
  220.7 44.3 %reduce-scatter.8.cloned.1.call-start = ((), (), s32[]{:S(2)}) async-start(), calls=%async_computation.6 | async-start | bytes 40960 | tf_op jit(solution)/shard_map/while/body/eval_jaxpr/reduce_scatter | solution.py:18
  265.8 3.9 collective-permute-start
  270.4 18.2 %all-to-all-start = ((bf16[32,32,96]{2,1,0:T(8,128)(2,1)}), bf16[32,32,96]{2,1,0:T(8,128)(2,1)S(1)}, u32[]{:S(2)}, u32[]{:S(2)}) async-start(bf16[32,32,96]{2,1,0:T(8,128)(2,1)} %stack.7), calls=%async_computation | async-start | bytes 524288 | tf_op jit(solution)/shard_map/while/body/eval_jaxpr/all_to_all | solution.py:163
  279.7 23.1 %reduce-scatter.4.cloned.1.call-start = ((), (), s32[]{:S(2)}) async-start(), calls=%async_computation.4 | async-start | bytes 393216 | tf_op jit(solution)/shard_map/while/body/eval_jaxpr/reduce_scatter | solution.py:18
  293.3 31.3 %reduce-scatter.6.cloned.1.call-start = ((), (), s32[]{:S(2)}) async-start(), calls=%async_computation.5 | async-start | bytes 163840 | tf_op jit(solution)/shard_map/while/body/eval_jaxpr/reduce_scatter | solution.py:18
  302.8 44.2 %reduce-scatter.8.cloned.1.call-start = ((), (), s32[]{:S(2)}) async-start(), calls=%async_computation.6 | async-start | bytes 40960 | tf_op jit(solution)/shard_map/while/body/eval_jaxpr/reduce_scatter | solution.py:18
  347.7 3.9 collective-permute-start
  352.3 18.2 %all-to-all-start = ((bf16[32,32,96]{2,1,0:T(8,128)(2,1)}), bf16[32,32,96]{2,1,0:T(8,128)(2,1)S(1)}, u32[]{:S(2)}, u32[]{:S(2)}) async-start(bf16[32,32,96]{2,1,0:T(8,128)(2,1)} %stack.7), calls=%async_computation | async-start | bytes 524288 | tf_op jit(solution)/shard_map/while/body/eval_jaxpr/all_to_all | solution.py:163
  361.6 23.1 %reduce-scatter.4.cloned.1.call-start = ((), (), s32[]{:S(2)}) async-start(), calls=%async_computation.4 | async-start | bytes 393216 | tf_op jit(solution)/shard_map/while/body/eval_jaxpr/reduce_scatter | solution.py:18
  375.2 31.2 %reduce-scatter.6.cloned.1.call-start = ((), (), s32[]{:S(2)}) async-start(), calls=%async_computation.5 | async-start | bytes 163840 | tf_op jit(solution)/shard_map/while/body/eval_jaxpr/reduce_scatter | solution.py:18
  384.7 44.0 %reduce-scatter.8.cloned.1.call-start = ((), (), s32[]{:S(2)}) async-start(), calls=%async_computation.6 | async-start | bytes 40960 | tf_op jit(solution)/shard_map/while/body/eval_jaxpr/reduce_scatter | solution.py:18
  429.4 3.9 collective-permute-start
Sparse Core Ops, SparseCore 0:
  48.8 7.9 reduce-scatter.3
  59.2 19.4 reduce-scatter.5
  81.0 20.1 reduce-scatter.7
  129.6 9.3 reduce-scatter.3
  141.2 19.4 reduce-scatter.5
  162.8 20.1 reduce-scatter.7
  211.3 9.3 reduce-scatter.3
  223.1 19.4 reduce-scatter.5
  244.9 20.1 reduce-scatter.7
  293.4 9.3 reduce-scatter.3
  305.1 19.4 reduce-scatter.5
  326.8 20.1 reduce-scatter.7
  375.3 9.3 reduce-scatter.3
  386.9 19.4 reduce-scatter.5
  408.6 20.1 reduce-scatter.7
